TPU v7x, 32 devices: a whole 2x2x4 slice. The times are simulated.
32 devices in a mesh: kv: 8 (over z, y), tp: 4 (over x, core).
Axes of the slice: x: 2, y: 2, z: 4, core: 2. Of those that a mesh axis runs over, the one named last changes fastest.
Arguments:
- tokens: bfloat16 [128, 4096], P('tp', 'kv')
- seq_pos: int32 [128], P('kv'), may hold values from 0 to 4095
- state: float32 [128, 16, 128, 256], P('kv', 'tp'), may hold values from -0.6 to 0.6
- norm_in_gain: float32 [4096], P('kv'), may hold values from 0.1 to 1.9
- query_weight: bfloat16 [4096, 2048], P('kv', 'tp'), may hold values from -0.09375 to 0.09375
- key_weight: bfloat16 [4096, 2048], P('kv', 'tp'), may hold values from -0.09375 to 0.09375
- value_weight: bfloat16 [4096, 4096], P('kv', 'tp'), may hold values from -0.09375 to 0.09375
- gate_weight: bfloat16 [4096, 4096], P('kv', 'tp'), may hold values from -0.09375 to 0.09375
- head_gain: float32 [4096], P('tp'), may hold values from 0.1 to 1.9
- out_weight: bfloat16 [4096, 4096], P('tp', 'kv'), may hold values from -0.09375 to 0.09375
- norm_mlp_gain: float32 [4096], P('kv'), may hold values from 0.1 to 1.9
- hidden_weight: bfloat16 [4096, 16384], P('kv', 'tp'), may hold values from -0.09375 to 0.09375
- down_weight: bfloat16 [16384, 4096], P('tp', 'kv'), may hold values from -0.046875 to 0.046875
Outputs:
- output: bfloat16 [128, 4096], P('tp', 'kv')
- new_state: float32 [128, 16, 128, 256], P('kv', 'tp')
All inputs are finite; a program needn't handle non-finite values.
Results may differ from a plain program's by a relative error of at most 0.03.
Values may be sent and summed in bfloat16 or wider, within the bound.
A program may use at most 64 MiB of HBM per device.

v0:
```python
import jax
import jax.numpy as jnp
from jax import lax
from jax.sharding import PartitionSpec as P

D = 4096
H = 16
DK = 128
DV = 256
EPS = 1e-06


def rotate(vectors, positions):
    half = vectors.shape[-1] // 2
    inverse = jnp.power(10000.0, -jnp.arange(half, dtype=jnp.float32) / half)
    angles = positions.astype(jnp.float32)[:, None] * inverse[None, :]
    cosine = jnp.cos(angles)[:, None, :]
    sine = jnp.sin(angles)[:, None, :]
    first, second = (vectors[..., :half], vectors[..., half:])
    return jnp.concatenate(
        [first * cosine - second * sine, first * sine + second * cosine], axis=-1
    )


def head_decay(head_ids):
    return 1.0 - jnp.exp2(-2.0 - 6.0 * head_ids / (H - 1))


def local(
    tokens,
    seq_pos,
    state,
    norm_in_gain,
    query_weight,
    key_weight,
    value_weight,
    gate_weight,
    head_gain,
    out_weight,
    norm_mlp_gain,
    hidden_weight,
    down_weight,
):
    rows_all = lax.all_gather(tokens, "tp", axis=0, tiled=True)
    rows_f = rows_all.astype(jnp.float32)
    squares_in = jnp.sum(rows_f * rows_f, axis=1)
    normed_in = (rows_f * norm_in_gain[None, :]).astype(jnp.bfloat16)
    term_query = jnp.dot(normed_in, query_weight, preferred_element_type=jnp.float32).astype(
        jnp.bfloat16
    )
    term_keys = jnp.dot(normed_in, key_weight, preferred_element_type=jnp.float32).astype(
        jnp.bfloat16
    )
    term_values = jnp.dot(normed_in, value_weight, preferred_element_type=jnp.float32).astype(
        jnp.bfloat16
    )
    term_gates = jnp.dot(normed_in, gate_weight, preferred_element_type=jnp.float32).astype(
        jnp.bfloat16
    )
    total_all = lax.psum(squares_in, "kv")
    query, keys, values, gates = (
        lax.psum_scatter(term_query, "kv", scatter_dimension=0, tiled=True).astype(jnp.float32),
        lax.psum_scatter(term_keys, "kv", scatter_dimension=0, tiled=True).astype(jnp.float32),
        lax.psum_scatter(term_values, "kv", scatter_dimension=0, tiled=True).astype(jnp.float32),
        lax.psum_scatter(term_gates, "kv", scatter_dimension=0, tiled=True).astype(jnp.float32),
    )
    own_rows = query.shape[0]
    total_in = lax.dynamic_slice_in_dim(total_all, lax.axis_index("kv") * own_rows, own_rows, 0)
    factor = lax.rsqrt(total_in / D + EPS)[:, None]
    query, keys, values, gates = (query * factor, keys * factor, values * factor, gates * factor)
    local_rows = query.shape[0]
    heads_dev = H // lax.axis_size("tp")
    turned_query = rotate(query.reshape(local_rows, heads_dev, DK), seq_pos)
    turned_keys = rotate(keys.reshape(local_rows, heads_dev, DK), seq_pos) * DK ** (-0.5)
    head_ids = (lax.axis_index("tp") * heads_dev + jnp.arange(heads_dev, dtype=jnp.int32)).astype(
        jnp.float32
    )
    decay = head_decay(head_ids)
    new_state = decay[None, :, None, None] * state + jnp.einsum(
        "bhk,bhv->bhkv",
        turned_keys,
        values.reshape(local_rows, heads_dev, DV),
        precision=lax.Precision.HIGHEST,
    )
    read = jnp.einsum("bhk,bhkv->bhv", turned_query, new_state, precision=lax.Precision.HIGHEST)
    read = read * lax.rsqrt(jnp.mean(read * read, axis=-1, keepdims=True) + EPS)
    mixed = (
        read.reshape(local_rows, heads_dev * DV) * head_gain[None, :] * jax.nn.silu(gates)
    ).astype(jnp.bfloat16)
    attn_terms = jnp.dot(
        lax.all_gather(mixed, "kv", axis=0, tiled=True),
        out_weight,
        preferred_element_type=jnp.float32,
    )
    attn = lax.psum_scatter(
        attn_terms.astype(jnp.bfloat16), "tp", scatter_dimension=0, tiled=True
    ).astype(jnp.float32)
    resid = (tokens.astype(jnp.float32) + attn).astype(jnp.bfloat16)
    resid_all = lax.all_gather(resid, "tp", axis=0, tiled=True)
    resid_f = resid_all.astype(jnp.float32)
    squares_mid = jnp.sum(resid_f * resid_f, axis=1)
    normed_mid = (resid_f * norm_mlp_gain[None, :]).astype(jnp.bfloat16)
    term_hidden = jnp.dot(normed_mid, hidden_weight, preferred_element_type=jnp.float32).astype(
        jnp.bfloat16
    )
    total_mid = lax.psum(squares_mid, "kv")
    scale_mid = lax.rsqrt(total_mid / D + EPS)[:, None]
    hidden = lax.psum(term_hidden, "kv").astype(jnp.float32)
    active = jnp.square(jax.nn.relu(hidden * scale_mid)).astype(jnp.bfloat16)
    down_terms = jnp.dot(active, down_weight, preferred_element_type=jnp.float32)
    down = lax.psum_scatter(
        down_terms.astype(jnp.bfloat16), "tp", scatter_dimension=0, tiled=True
    ).astype(jnp.float32)
    output = (resid.astype(jnp.float32) + down).astype(jnp.bfloat16)
    return (output, new_state)


def solution(mesh):
    placed = (
        P("tp", "kv"),
        P("kv"),
        P("kv", "tp", None, None),
        P("kv"),
        P("kv", "tp"),
        P("kv", "tp"),
        P("kv", "tp"),
        P("kv", "tp"),
        P("tp"),
        P("tp", "kv"),
        P("kv"),
        P("kv", "tp"),
        P("tp", "kv"),
    )
    return jax.shard_map(
        local,
        mesh=mesh,
        in_specs=placed,
        out_specs=(P("tp", "kv"), P("kv", "tp", None, None)),
        check_vma=False,
    )
```

profile of v0, /device:TPU:0, one launch (start us, length us, event | category | flops | bytes accessed | tf_op | source)
XLA Modules:
  0.0 445.5 jit_solution(3664040884219889815)
XLA Ops:
  7.2 6.9 %all_gather.9 = bf16[128,512]{1,0:T(8,128)(2,1)S(1)} all-gather(bf16[32,512]{1,0:T(8,128)(2,1)} %param.13), channel_id=1, replica_groups=mesh['kv'=8,'tp'=4] {'tp'}, dimensions={0}, use_global_device_ids=true | all-gather | bytes 163840 | tf_op jit(solution)/shard_map/all_gather | solution.py:44
  14.1 2.0 convolution_convert_fusion.4
  16.1 1.9 convolution_convert_fusion.5
  18.1 1.7 convolution_convert_fusion.2
  19.9 2.2 convolution_convert_fusion.1
  22.4 22.1 %psum.21 = f32[128]{0:T(128)S(1)} all-reduce(f32[128]{0:T(128)S(1)} %fusion.3), channel_id=1, replica_groups=mesh['kv'=8,'tp'=4] {'kv'}, use_global_device_ids=true, to_apply=%region_2.0 | all-reduce | flops 128 | bytes 1024 | tf_op jit(solution)/shard_map/psum | solution.py:60
  44.7 35.0 %reduce-scatter.9.cloned.1.call-done = bf16[16,512]{1,0:T(8,128)(2,1)} async-done(((bf16[128,512]{1,0:T(8,128)(2,1)}), bf16[16,512]{1,0:T(8,128)(2,1)}) %reduce-scatter.9.cloned.1.call-update) | async-done | bytes 16400 | tf_op jit(solution)/shard_map/reduce_scatter | solution.py:63
  79.7 64.2 %reduce-scatter.7.cloned.1.call-done = bf16[16,512]{1,0:T(8,128)(2,1)} async-done(((bf16[128,512]{1,0:T(8,128)(2,1)}), bf16[16,512]{1,0:T(8,128)(2,1)}) %reduce-scatter.7.cloned.1.call-update) | async-done | bytes 16400 | tf_op jit(solution)/shard_map/reduce_scatter | solution.py:62
  144.9 64.0 %reduce-scatter.11.cloned.1.call-done = bf16[16,1024]{1,0:T(8,128)(2,1)} async-done(((bf16[128,1024]{1,0:T(8,128)(2,1)}), bf16[16,1024]{1,0:T(8,128)(2,1)}) %reduce-scatter.11.cloned.1.call-update) | async-done | bytes 32784 | tf_op jit(solution)/shard_map/reduce_scatter | solution.py:64
  208.9 0.8 convert_multiply_fusion.4
  209.7 4.1 multiply_add_fusion
  213.9 4.1 fusion.14
  218.3 55.3 %reduce-scatter.13.cloned.1.call-done = bf16[16,1024]{1,0:T(8,128)(2,1)} async-done(((bf16[128,1024]{1,0:T(8,128)(2,1)}), bf16[16,1024]{1,0:T(8,128)(2,1)}) %reduce-scatter.13.cloned.1.call-update) | async-done | bytes 32784 | tf_op jit(solution)/shard_map/reduce_scatter | solution.py:65
  273.6 0.9 multiply_convert_fusion.2
  274.4 30.9 %all_gather.10 = bf16[128,1024]{1,0:T(8,128)(2,1)S(1)} all-gather(bf16[16,1024]{1,0:T(8,128)(2,1)S(1)} %multiply_convert_fusion.2), channel_id=1, replica_groups=mesh['kv'=8,'tp'=4] {'kv'}, dimensions={0}, use_global_device_ids=true | all-gather | bytes 294912 | tf_op jit(solution)/shard_map/all_gather | solution.py:91
  305.3 1.0 convolution_convert_fusion.6
  306.4 18.8 %reduce-scatter.15.cloned.1.call-done = bf16[32,512]{1,0:T(8,128)(2,1)} async-done(((bf16[128,512]{1,0:T(8,128)(2,1)}), bf16[32,512]{1,0:T(8,128)(2,1)}) %reduce-scatter.15.cloned.1.call-update) | async-done | bytes 32784 | tf_op jit(solution)/shard_map/reduce_scatter | solution.py:95
  325.9 5.4 %all_gather.11 = bf16[128,512]{1,0:T(8,128)(2,1)S(1)} all-gather(bf16[32,512]{1,0:T(8,128)(2,1)S(1)} %add_convert_fusion.1), channel_id=1, replica_groups=mesh['kv'=8,'tp'=4] {'tp'}, dimensions={0}, use_global_device_ids=true | all-gather | bytes 163840 | tf_op jit(solution)/shard_map/all_gather | solution.py:99
  331.3 3.9 convolution_convert_fusion
  335.5 21.6 %psum.23 = f32[128]{0:T(128)S(1)} all-reduce(f32[128]{0:T(128)S(1)} %fusion.5), channel_id=1, replica_groups=mesh['kv'=8,'tp'=4] {'kv'}, use_global_device_ids=true, to_apply=%region_10.11 | all-reduce | flops 128 | bytes 1024 | tf_op jit(solution)/shard_map/psum | solution.py:106
  357.1 56.9 %all-reduce.2.cloned.1.call-done = bf16[128,4096]{1,0:T(8,128)(2,1)} async-done(((bf16[128,4096]{1,0:T(8,128)(2,1)}), bf16[128,4096]{1,0:T(8,128)(2,1)}) %all-reduce.2.cloned.1.call-update) | async-done | bytes 1048592 | tf_op jit(solution)/shard_map/psum | solution.py:108
  414.0 3.9 convolution_convert_fusion.3
  417.9 19.4 %reduce-scatter.17.cloned.1.call-done = bf16[32,512]{1,0:T(8,128)(2,1)} async-done(((bf16[128,512]{1,0:T(8,128)(2,1)}), bf16[32,512]{1,0:T(8,128)(2,1)}) %reduce-scatter.17.cloned.1.call-update) | async-done | bytes 32784 | tf_op jit(solution)/shard_map/reduce_scatter | solution.py:111
  437.3 1.4 add_convert_fusion
  (47 shorter events, 2.9 us)
Async XLA Ops:
  7.2 11.0 %copy-start = (bf16[512,1024]{1,0:T(8,128)(2,1)S(1)}, bf16[512,1024]{1,0:T(8,128)(2,1)}, u32[]{:S(2)}) copy-start(bf16[512,1024]{1,0:T(8,128)(2,1)} %param.19) | copy-start | bytes 3145732
  7.2 15.2 %copy-start.6 = (s32[16]{0:T(128)S(1)}, s32[16]{0:T(128)}, u32[]{:S(2)}) copy-start(s32[16]{0:T(128)} %param.14) | copy-start | bytes 196
  7.2 72.5 %reduce-scatter.9.cloned.1.call-start = ((), (), s32[]{:S(2)}) async-start(), calls=%async_computation.7 | async-start | bytes 147456 | tf_op jit(solution)/shard_map/reduce_scatter | solution.py:63
  16.1 127.8 %reduce-scatter.7.cloned.1.call-start = ((), (), s32[]{:S(2)}) async-start(), calls=%async_computation.6 | async-start | bytes 147456 | tf_op jit(solution)/shard_map/reduce_scatter | solution.py:62
  18.1 190.8 %reduce-scatter.11.cloned.1.call-start = ((), (), s32[]{:S(2)}) async-start(), calls=%async_computation.8 | async-start | bytes 294912 | tf_op jit(solution)/shard_map/reduce_scatter | solution.py:64
  19.9 253.7 %reduce-scatter.13.cloned.1.call-start = ((), (), s32[]{:S(2)}) async-start(), calls=%async_computation.9 | async-start | bytes 294912 | tf_op jit(solution)/shard_map/reduce_scatter | solution.py:65
  22.2 303.0 %reduce-scatter.15.cloned.1.call-start = ((), (), s32[]{:S(2)}) async-start(), calls=%async_computation.10 | async-start | bytes 163840 | tf_op jit(solution)/shard_map/reduce_scatter | solution.py:95
  213.9 4.1 copy-start.1
  213.9 59.7 %copy-start.4 = (f32[1024]{0:T(1024)S(1)}, f32[1024]{0:T(1024)}, u32[]{:S(2)}) copy-start(f32[1024]{0:T(1024)} %param.21) | copy-start | bytes 12292
  213.9 91.4 %copy-start.2 = (bf16[1024,512]{1,0:T(8,128)(2,1)S(1)}, bf16[1024,512]{1,0:T(8,128)(2,1)}, u32[]{:S(2)}) copy-start(bf16[1024,512]{1,0:T(8,128)(2,1)} %param.22) | copy-start | bytes 3145732
  213.9 111.2 %copy-start.3 = (bf16[32,512]{1,0:T(8,128)(2,1)S(1)}, bf16[32,512]{1,0:T(8,128)(2,1)}, u32[]{:S(2)}) copy-start(bf16[32,512]{1,0:T(8,128)(2,1)} %param.13) | copy-start | bytes 98308
  213.9 117.4 %copy-start.5 = (f32[512]{0:T(512)S(1)}, f32[512]{0:T(512)}, u32[]{:S(2)}) copy-start(f32[512]{0:T(512)} %param.23) | copy-start | bytes 6148
  306.3 107.6 %all-reduce.2.cloned.1.call-start = ((), (), s32[]{:S(2)}) async-start(), calls=%async_computation.11 | async-start | bytes 2097152 | tf_op jit(solution)/shard_map/psum | solution.py:108
  335.3 102.0 %reduce-scatter.17.cloned.1.call-start = ((), (), s32[]{:S(2)}) async-start(), calls=%async_computation.12 | async-start | bytes 163840 | tf_op jit(solution)/shard_map/reduce_scatter | solution.py:111
Sparse Core Ops, SparseCore 0:
  16.2 63.4 reduce-scatter.8
  83.0 60.8 reduce-scatter.6
  147.8 61.0 reduce-scatter.10
  212.1 61.4 reduce-scatter.12
  306.5 18.6 reduce-scatter.14
  335.4 78.4 all-reduce.1
  418.0 19.2 reduce-scatter.16
where the time goes:
time: 446 us
  waiting for transfers between devices  314 us (70%)
  blocking collectives  86.9 us (19%)
  matrix products  20.8 us (5%)
  between operations  14.3 us (3%)
  other arithmetic  9.62 us (2%)
    reduce_scatter x1, waiting for transfers between devices, local(): lax.psum_scatter(term_query, 'kv', scatter_dimension=0, tiled=True)  64.2 us
    reduce_scatter x1, waiting for transfers between devices, local(): lax.psum_scatter(term_values, 'kv', scatter_dimension=0, tiled=True)  64 us
    psum x1, waiting for transfers between devices, local(): hidden = lax.psum(term_hidden, 'kv').astype(jnp.float32)  56.9 us
    reduce_scatter x1, waiting for transfers between devices, local(): lax.psum_scatter(term_gates, 'kv', scatter_dimension=0, tiled=True)  55.3 us
    reduce_scatter x1, waiting for transfers between devices, local(): lax.psum_scatter(term_keys, 'kv', scatter_dimension=0, tiled=True)  35 us
    all_gather x1, blocking collectives, local(): lax.all_gather(mixed, 'kv', axis=0, tiled=True)  30.9 us
    psum x1, blocking collectives, local(): total_all = lax.psum(squares_in, 'kv')  22.1 us
    psum x1, blocking collectives, local(): total_mid = lax.psum(squares_mid, 'kv')  21.6 us
  transfers between devices with their start and end apart: 7, of which 7 were waited for; matrix products, arithmetic and copies ran while one was open for 4% of the time, Pallas kernels for 0%

commit v1 on v0

--- a/solution.py
+++ b/solution.py
@@ -88,7 +88,9 @@
         read.reshape(local_rows, heads_dev * DV) * head_gain[None, :] * jax.nn.silu(gates)
     ).astype(jnp.bfloat16)
     attn_terms = jnp.dot(
-        lax.all_gather(mixed, "kv", axis=0, tiled=True),
+        jnp.concatenate(
+            lax.all_to_all(jnp.stack([mixed] * lax.axis_size("kv")), "kv", 0, 0), axis=0
+        ),
         out_weight,
         preferred_element_type=jnp.float32,
     )

time: 446 us -> 426 us (0.955)
  blocking collectives: 86.9 us -> 67.6 us
    all_gather x1 -> x0, blocking collectives: 30.9 us -> none  [local(): lax.all_gather(mixed, 'kv', axis=0, tiled=True)]
    all_to_all x0 -> x1, blocking collectives: none -> 11.7 us  [local(): lax.all_to_all(jnp.stack([mixed] * lax.axis_size('kv')), 'kv', 0, 0)]
where the time goes in v1:
time: 426 us
  waiting for transfers between devices  313 us (73%)
  blocking collectives  67.6 us (16%)
  matrix products  20.8 us (5%)
  between operations  14.3 us (3%)
  other arithmetic  9.62 us (2%)
    reduce_scatter x1, waiting for transfers between devices, local(): lax.psum_scatter(term_query, 'kv', scatter_dimension=0, tiled=True)  64.2 us
    reduce_scatter x1, waiting for transfers between devices, local(): lax.psum_scatter(term_values, 'kv', scatter_dimension=0, tiled=True)  64 us
    psum x1, waiting for transfers between devices, local(): hidden = lax.psum(term_hidden, 'kv').astype(jnp.float32)  56.8 us
    reduce_scatter x1, waiting for transfers between devices, local(): lax.psum_scatter(term_gates, 'kv', scatter_dimension=0, tiled=True)  55.3 us
    reduce_scatter x1, waiting for transfers between devices, local(): lax.psum_scatter(term_keys, 'kv', scatter_dimension=0, tiled=True)  35 us
    psum x1, blocking collectives, local(): total_all = lax.psum(squares_in, 'kv')  22.1 us
    psum x1, blocking collectives, local(): total_mid = lax.psum(squares_mid, 'kv')  21.6 us
    reduce_scatter x1, waiting for transfers between devices, local(): lax.psum_scatter(down_terms.astype(jnp.bfloat16), 'tp', scatter_dimension...  19.4 us
  transfers between devices with their start and end apart: 7, of which 7 were waited for; matrix products, arithmetic and copies ran while one was open for 4% of the time, Pallas kernels for 0%

profile of v1, /device:TPU:0, one launch (start us, length us, event | category | flops | bytes accessed | tf_op | source)
XLA Modules:
  0.0 425.5 jit_solution(82238309147636796)
XLA Ops:
  7.2 6.9 %all_gather.6 = bf16[128,512]{1,0:T(8,128)(2,1)S(1)} all-gather(bf16[32,512]{1,0:T(8,128)(2,1)} %param.13), channel_id=1, replica_groups=mesh['kv'=8,'tp'=4] {'tp'}, dimensions={0}, use_global_device_ids=true | all-gather | bytes 163840 | tf_op jit(solution)/shard_map/all_gather | solution.py:44
  14.1 2.0 convolution_convert_fusion.4
  16.1 1.9 convolution_convert_fusion.5
  18.1 1.7 convolution_convert_fusion.2
  19.9 2.2 convolution_convert_fusion.1
  22.4 22.1 %psum.21 = f32[128]{0:T(128)S(1)} all-reduce(f32[128]{0:T(128)S(1)} %fusion.3), channel_id=1, replica_groups=mesh['kv'=8,'tp'=4] {'kv'}, use_global_device_ids=true, to_apply=%region_2.0 | all-reduce | flops 128 | bytes 1024 | tf_op jit(solution)/shard_map/psum | solution.py:60
  44.7 35.0 %reduce-scatter.9.cloned.1.call-done = bf16[16,512]{1,0:T(8,128)(2,1)} async-done(((bf16[128,512]{1,0:T(8,128)(2,1)}), bf16[16,512]{1,0:T(8,128)(2,1)}) %reduce-scatter.9.cloned.1.call-update) | async-done | bytes 16400 | tf_op jit(solution)/shard_map/reduce_scatter | solution.py:63
  79.7 64.2 %reduce-scatter.7.cloned.1.call-done = bf16[16,512]{1,0:T(8,128)(2,1)} async-done(((bf16[128,512]{1,0:T(8,128)(2,1)}), bf16[16,512]{1,0:T(8,128)(2,1)}) %reduce-scatter.7.cloned.1.call-update) | async-done | bytes 16400 | tf_op jit(solution)/shard_map/reduce_scatter | solution.py:62
  144.9 64.0 %reduce-scatter.11.cloned.1.call-done = bf16[16,1024]{1,0:T(8,128)(2,1)} async-done(((bf16[128,1024]{1,0:T(8,128)(2,1)}), bf16[16,1024]{1,0:T(8,128)(2,1)}) %reduce-scatter.11.cloned.1.call-update) | async-done | bytes 32784 | tf_op jit(solution)/shard_map/reduce_scatter | solution.py:64
  208.9 0.8 convert_multiply_fusion.4
  209.7 4.1 multiply_add_fusion
  213.9 4.1 fusion.14
  218.3 55.3 %reduce-scatter.13.cloned.1.call-done = bf16[16,1024]{1,0:T(8,128)(2,1)} async-done(((bf16[128,1024]{1,0:T(8,128)(2,1)}), bf16[16,1024]{1,0:T(8,128)(2,1)}) %reduce-scatter.13.cloned.1.call-update) | async-done | bytes 32784 | tf_op jit(solution)/shard_map/reduce_scatter | solution.py:65
  273.6 0.9 multiply_convert_fusion.2
  274.5 11.7 %all_to_all.5 = bf16[8,16,1024]{2,1,0:T(8,128)(2,1)S(1)} all-to-all(bf16[8,16,1024]{2,1,0:T(8,128)(2,1)S(1)} %stack.2), channel_id=1, replica_groups=mesh['kv'=8,'tp'=4] {'kv'}, dimensions={0} | all-to-all | bytes 524288 | tf_op jit(solution)/shard_map/all_to_all | solution.py:92
  286.1 1.0 convolution_convert_fusion.6
  287.2 18.0 %reduce-scatter.15.cloned.1.call-done = bf16[32,512]{1,0:T(8,128)(2,1)} async-done(((bf16[128,512]{1,0:T(8,128)(2,1)}), bf16[32,512]{1,0:T(8,128)(2,1)}) %reduce-scatter.15.cloned.1.call-update) | async-done | bytes 32784 | tf_op jit(solution)/shard_map/reduce_scatter | solution.py:97
  306.0 5.4 %all_gather.7 = bf16[128,512]{1,0:T(8,128)(2,1)S(1)} all-gather(bf16[32,512]{1,0:T(8,128)(2,1)S(1)} %add_convert_fusion.1), channel_id=1, replica_groups=mesh['kv'=8,'tp'=4] {'tp'}, dimensions={0}, use_global_device_ids=true | all-gather | bytes 163840 | tf_op jit(solution)/shard_map/all_gather | solution.py:101
  311.4 3.9 convolution_convert_fusion
  315.5 21.6 %psum.23 = f32[128]{0:T(128)S(1)} all-reduce(f32[128]{0:T(128)S(1)} %fusion.5), channel_id=1, replica_groups=mesh['kv'=8,'tp'=4] {'kv'}, use_global_device_ids=true, to_apply=%region_10.11 | all-reduce | flops 128 | bytes 1024 | tf_op jit(solution)/shard_map/psum | solution.py:108
  337.1 56.8 %all-reduce.2.cloned.1.call-done = bf16[128,4096]{1,0:T(8,128)(2,1)} async-done(((bf16[128,4096]{1,0:T(8,128)(2,1)}), bf16[128,4096]{1,0:T(8,128)(2,1)}) %all-reduce.2.cloned.1.call-update) | async-done | bytes 1048592 | tf_op jit(solution)/shard_map/psum | solution.py:110
  394.0 3.9 convolution_convert_fusion.3
  397.9 19.4 %reduce-scatter.17.cloned.1.call-done = bf16[32,512]{1,0:T(8,128)(2,1)} async-done(((bf16[128,512]{1,0:T(8,128)(2,1)}), bf16[32,512]{1,0:T(8,128)(2,1)}) %reduce-scatter.17.cloned.1.call-update) | async-done | bytes 32784 | tf_op jit(solution)/shard_map/reduce_scatter | solution.py:113
  417.3 1.4 add_convert_fusion
  (48 shorter events, 3.0 us)
Async XLA Ops:
  7.2 11.0 %copy-start = (bf16[512,1024]{1,0:T(8,128)(2,1)S(1)}, bf16[512,1024]{1,0:T(8,128)(2,1)}, u32[]{:S(2)}) copy-start(bf16[512,1024]{1,0:T(8,128)(2,1)} %param.19) | copy-start | bytes 3145732
  7.2 15.2 %copy-start.6 = (s32[16]{0:T(128)S(1)}, s32[16]{0:T(128)}, u32[]{:S(2)}) copy-start(s32[16]{0:T(128)} %param.14) | copy-start | bytes 196
  7.2 72.5 %reduce-scatter.9.cloned.1.call-start = ((), (), s32[]{:S(2)}) async-start(), calls=%async_computation.8 | async-start | bytes 147456 | tf_op jit(solution)/shard_map/reduce_scatter | solution.py:63
  16.1 127.8 %reduce-scatter.7.cloned.1.call-start = ((), (), s32[]{:S(2)}) async-start(), calls=%async_computation.7 | async-start | bytes 147456 | tf_op jit(solution)/shard_map/reduce_scatter | solution.py:62
  18.1 190.8 %reduce-scatter.11.cloned.1.call-start = ((), (), s32[]{:S(2)}) async-start(), calls=%async_computation.9 | async-start | bytes 294912 | tf_op jit(solution)/shard_map/reduce_scatter | solution.py:64
  19.9 253.7 %reduce-scatter.13.cloned.1.call-start = ((), (), s32[]{:S(2)}) async-start(), calls=%async_computation.10 | async-start | bytes 294912 | tf_op jit(solution)/shard_map/reduce_scatter | solution.py:65
  22.2 283.0 %reduce-scatter.15.cloned.1.call-start = ((), (), s32[]{:S(2)}) async-start(), calls=%async_computation.11 | async-start | bytes 163840 | tf_op jit(solution)/shard_map/reduce_scatter | solution.py:97
  213.9 4.1 copy-start.1
  213.9 59.7 %copy-start.4 = (f32[1024]{0:T(1024)S(1)}, f32[1024]{0:T(1024)}, u32[]{:S(2)}) copy-start(f32[1024]{0:T(1024)} %param.21) | copy-start | bytes 12292
  213.9 72.2 %copy-start.2 = (bf16[1024,512]{1,0:T(8,128)(2,1)S(1)}, bf16[1024,512]{1,0:T(8,128)(2,1)}, u32[]{:S(2)}) copy-start(bf16[1024,512]{1,0:T(8,128)(2,1)} %param.22) | copy-start | bytes 3145732
  213.9 91.3 %copy-start.3 = (bf16[32,512]{1,0:T(8,128)(2,1)S(1)}, bf16[32,512]{1,0:T(8,128)(2,1)}, u32[]{:S(2)}) copy-start(bf16[32,512]{1,0:T(8,128)(2,1)} %param.13) | copy-start | bytes 98308
  213.9 97.5 %copy-start.5 = (f32[512]{0:T(512)S(1)}, f32[512]{0:T(512)}, u32[]{:S(2)}) copy-start(f32[512]{0:T(512)} %param.23) | copy-start | bytes 6148
  287.1 106.9 %all-reduce.2.cloned.1.call-start = ((), (), s32[]{:S(2)}) async-start(), calls=%async_computation.12 | async-start | bytes 2097152 | tf_op jit(solution)/shard_map/psum | solution.py:110
  315.4 101.9 %reduce-scatter.17.cloned.1.call-start = ((), (), s32[]{:S(2)}) async-start(), calls=%async_computation.13 | async-start | bytes 163840 | tf_op jit(solution)/shard_map/reduce_scatter | solution.py:113
Sparse Core Ops, SparseCore 0:
  16.2 63.4 reduce-scatter.8
  83.0 60.8 reduce-scatter.6
  147.8 61.0 reduce-scatter.10
  212.1 61.4 reduce-scatter.12
  287.2 17.9 reduce-scatter.14
  315.5 78.4 all-reduce.1
  398.0 19.2 reduce-scatter.16
